TPU v7x, 32 devices: a whole 2x2x4 slice. The times are simulated.
32 devices in a mesh: grp: 2 (over y), fs: 4 (over z), tp: 4 (over x, core).
Axes of the slice: x: 2, y: 2, z: 4, core: 2. Of those that a mesh axis runs over, the one named last changes fastest.
Arguments:
- prompt_rows: bfloat16 [8192, 2048], P(('grp', 'fs')), parts along dimension 0, may hold values from -6 to 6
- up_master: float32 [2048, 8192], P('fs', 'tp'), may hold values from -0.125 to 0.125
- down_master: float32 [8192, 2048], P('fs', 'tp'), may hold values from -0.0625 to 0.0625
- norm_gain: float32 [2048], P('fs'), may hold values from 0.1 to 1.9
Outputs:
- up_sampler: bfloat16 [8, 2048, 2048], P(('grp', 'tp')), parts along dimension 0
- down_sampler: bfloat16 [8, 2048, 2048], P(('grp', 'tp')), parts along dimension 0
- layer_out: bfloat16 [8192, 2048], P(('grp', 'fs', 'tp')), parts along dimension 0
There are 2 independent parts, one for each index of `grp`. A program takes and returns all parts, laid end to end along the dimension named above; an argument that names none is the same for every part. Nothing has to cross between parts.
All inputs are finite; a program needn't handle non-finite values.
Results may differ from a plain program's by a relative error of at most 0.014.
Values may be sent and summed in bfloat16 or wider, within the bound.
A program may use at most 128 MiB of HBM per device.

v0:
```python
import jax
import jax.numpy as jnp
from jax import lax
from jax.sharding import PartitionSpec as P

eps = 1e-06


def on_device(prompt_rows, up_master, down_master, norm_gain):
    fs_count = lax.axis_size("fs")
    tp_count = lax.axis_size("tp")
    fs_per_tp = fs_count // tp_count
    up_cast = (up_master * norm_gain[:, None]).astype(jnp.bfloat16)
    down_cast = down_master.astype(jnp.bfloat16)
    up_local_rows = up_cast.shape[0]
    local_width = up_cast.shape[1]
    unit_span = local_width // fs_count
    down_local_cols = down_cast.shape[1]
    full_width = down_local_cols * tp_count
    values = prompt_rows.astype(jnp.float32)
    normed = (values * lax.rsqrt(jnp.mean(values * values, axis=-1, keepdims=True) + eps)).astype(
        jnp.bfloat16
    )
    up_parts = up_cast.reshape(up_local_rows, fs_per_tp, tp_count, unit_span)
    up_local = lax.all_to_all(up_parts, "tp", split_axis=2, concat_axis=1, tiled=True).reshape(
        up_local_rows, local_width
    )
    up_sampler = lax.all_gather(up_local, "fs", axis=0, tiled=True)
    down_parts = down_cast.reshape(tp_count, unit_span, down_local_cols)
    down_local = lax.all_to_all(down_parts, "tp", split_axis=0, concat_axis=2, tiled=True).reshape(
        unit_span, full_width
    )
    down_sampler = lax.all_gather(down_local, "fs", axis=0, tiled=True)
    pre_act = jnp.dot(normed, up_sampler, preferred_element_type=jnp.float32)
    hidden = jnp.square(jax.nn.relu(pre_act)).astype(jnp.bfloat16)
    summed = lax.psum_scatter(
        jnp.dot(hidden, down_sampler, preferred_element_type=jnp.float32).astype(jnp.bfloat16),
        "tp",
        scatter_dimension=0,
        tiled=True,
    )
    return (up_sampler[None], down_sampler[None], summed)


def solution(mesh):
    in_specs = (P(("grp", "fs"), None), P("fs", "tp"), P("fs", "tp"), P("fs"))
    out_specs = (
        P(("grp", "tp"), None, None),
        P(("grp", "tp"), None, None),
        P(("grp", "fs", "tp"), None),
    )
    return jax.shard_map(
        on_device, mesh=mesh, in_specs=in_specs, out_specs=out_specs, check_vma=False
    )
```

profile of v0, /device:TPU:1, one launch (start us, length us, event | category | flops | bytes accessed | tf_op | source)
XLA Modules:
  0.0 415.9 jit_solution(6983446177385879946)
XLA Ops:
  7.2 0.0 all-gather.5.cloned.1.call-start
  7.2 2.5 convert_element_type.19
  9.7 28.7 %all_to_all.24 = bf16[4,512,512]{2,1,0:T(8,128)(2,1)S(1)} all-to-all(bf16[4,512,512]{2,1,0:T(8,128)(2,1)S(1)} %bitcast.12), channel_id=1, replica_groups=mesh['grp'=2,'fs'=4,'tp'=4] {'tp'}, dimensions={0} | all-to-all | bytes 4194304 | tf_op jit(solution)/shard_map/all_to_all | solution.py:30
  38.4 2.4 copy.11
  40.7 0.0 all-gather.5.cloned.1.call-update
  40.7 0.0 copy-start
  40.7 0.0 all-gather.3.cloned.1.call-start
  40.8 5.3 %copy.8 = f32[512,2048]{0,1:T(8,128)} copy(f32[512,2048]{1,0:T(8,128)} %param.5) | data formatting | bytes 8388608 | tf_op args[1]
  46.1 0.0 copy-done
  46.1 2.8 multiply_convert_fusion.1
  48.9 2.4 copy.9
  51.3 30.0 %all_to_all.25 = bf16[512,1,4,512]{3,0,1,2:T(8,128)(2,1)S(1)} all-to-all(bf16[512,1,4,512]{3,0,1,2:T(8,128)(2,1)} %copy.9), channel_id=1, replica_groups=mesh['grp'=2,'fs'=4,'tp'=4] {'tp'}, dimensions={2} | all-to-all | bytes 4194304 | tf_op jit(solution)/shard_map/all_to_all | solution.py:25
  81.3 2.4 copy.10
  83.7 0.0 all-gather.3.cloned.1.call-update
  83.7 0.0 reduce-scatter.2.cloned.1.call-start
  83.7 3.1 fusion
  86.9 104.5 %all-gather.5.cloned.1.call-done = bf16[2048,2048]{0,1:T(8,128)(2,1)} async-done(((bf16[512,2048]{0,1:T(8,128)(2,1)}), bf16[2048,2048]{0,1:T(8,128)(2,1)}) %all-gather.5.cloned.1.call-update) | async-done | bytes 8388624 | tf_op jit(solution)/shard_map/all_gather | solution.py:33
  191.4 150.0 %all-gather.3.cloned.1.call-done = bf16[2048,2048]{0,1:T(8,128)(2,1)} async-done(((bf16[512,2048]{0,1:T(8,128)(2,1)}), bf16[2048,2048]{0,1:T(8,128)(2,1)}) %all-gather.3.cloned.1.call-update) | async-done | bytes 8388624 | tf_op jit(solution)/shard_map/all_gather | solution.py:28
  341.3 25.4 %fusion.9 = bf16[1024,2048]{1,0:T(8,128)(2,1)} fusion(bf16[2048,2048]{0,1:T(8,128)(2,1)} %all-gather.5.cloned.1.call-done, bf16[2048,2048]{0,1:T(8,128)(2,1)} %all-gather.3.cloned.1.call-done, bf16[1024,2048]{1,0:T(8,128)(2,1)} %param.4, f32[1024]{0:T(1024)S(1)} %add_rsqrt_fusion), kind=kOutput, calls=%fused_computation.9 | convolution fusion | flops 17194549248 | bytes 25169920 | tf_op jit(solution)/shard_map/dot_general | solution.py:37
  366.7 0.0 reduce-scatter.2.cloned.1.call-update
  366.8 12.4 %copy.12 = bf16[1,2048,2048]{2,1,0:T(8,128)(2,1)} copy(bf16[1,2048,2048]{1,2,0:T(8,128)(2,1)} %bitcast.14) | data formatting | bytes 16777216
  379.2 11.8 %copy.13 = bf16[1,2048,2048]{2,1,0:T(8,128)(2,1)} copy(bf16[1,2048,2048]{1,2,0:T(8,128)(2,1)} %bitcast.13) | data formatting | bytes 16777216
  391.0 18.4 %reduce-scatter.2.cloned.1.call-done = bf16[256,2048]{1,0:T(8,128)(2,1)} async-done(((bf16[1024,2048]{1,0:T(8,128)(2,1)}), bf16[256,2048]{1,0:T(8,128)(2,1)}) %reduce-scatter.2.cloned.1.call-update) | async-done | bytes 1048592 | tf_op jit(solution)/shard_map/reduce_scatter | solution.py:36
  (1 shorter events, 0.0 us)
Async XLA Ops:
  7.2 184.2 %all-gather.5.cloned.1.call-start = ((), (), s32[]{:S(2)}) async-start(), calls=%async_computation.4 | async-start | bytes 10485760 | tf_op jit(solution)/shard_map/all_gather | solution.py:33
  40.7 5.4 %copy-start = (f32[512]{0:T(512)S(1)}, f32[512]{0:T(512)}, u32[]{:S(2)}) copy-start(f32[512]{0:T(512)} %param.7) | copy-start | bytes 6148
  40.7 300.6 %all-gather.3.cloned.1.call-start = ((), (), s32[]{:S(2)}) async-start(), calls=%async_computation.3 | async-start | bytes 10485760 | tf_op jit(solution)/shard_map/all_gather | solution.py:28
  83.7 325.7 %reduce-scatter.2.cloned.1.call-start = ((), (), s32[]{:S(2)}) async-start(), calls=%async_computation.5 | async-start | bytes 5242880 | tf_op jit(solution)/shard_map/reduce_scatter | solution.py:36
Sparse Core Ops, SparseCore 0:
  40.8 150.4 all-gather.4
  193.5 147.7 all-gather.2
  366.9 42.4 reduce-scatter.1
where the time goes:
time: 418 us; the launch traced here: 416 us
  waiting for transfers between devices  273 us (65%)
  blocking collectives  58.7 us (14%)
  local copies, waits for them, and re-layouts  36.7 us (9%)
  matrix products  25.4 us (6%)
  between operations  13.8 us (3%)
  other arithmetic  8.34 us (2%)
    all_gather x1, waiting for transfers between devices, on_device(): up_sampler = lax.all_gather(up_local, 'fs', axis=0, tiled=True)  150 us
    all_gather x1, waiting for transfers between devices, on_device(): down_sampler = lax.all_gather(down_local, 'fs', axis=0, tiled=True)  104 us
    all_to_all x1, blocking collectives, on_device(): lax.all_to_all(up_parts, 'tp', split_axis=2, concat_axis=1, tiled=True)  30 us
    unnamed x5, local copies, waits for them, and re-layouts  29.6 us
    all_to_all x1, blocking collectives, on_device(): lax.all_to_all(down_parts, 'tp', split_axis=0, concat_axis=2, tiled=True)  28.7 us
    dot_general x1, matrix products, on_device(): jnp.dot(hidden, down_sampler, preferred_element_type=jnp.float32)  25.4 us
    reduce_scatter x1, waiting for transfers between devices, on_device(): lax.psum_scatter(jnp.dot(hidden, down_sampler, preferred_element_type=jnp...  18.4 us
  transfers between devices with their start and end apart: 3, of which 3 were waited for; matrix products, arithmetic and copies ran while one was open for 10% of the time, Pallas kernels for 0%

commit v1 on v0

v1 whole, which is shorter than its diff:
```python
import functools

import jax
import jax.numpy as jnp
from jax import lax
from jax.experimental import pallas as pl
from jax.experimental.pallas import tpu as pltpu
from jax.sharding import PartitionSpec as P

eps = 1e-06
row_tile = 256
norm_tile = 64
copy_rows = 256
copy_slots = 8
MESH = pl.DeviceIdType.MESH


def gather_kernel(
    n, tp, up_cast, down_cast, rows_ref, up_out, down_out, layer_out,
    up_all, down_all, normed, hidden, part, arrived,
    local_sem, tp_send, tp_recv, z_send, z_recv, y_send, y_recv,
    sum_send, sum_recv, out_sem,
):
    y = lax.axis_index("grp")
    z = lax.axis_index("fs")
    me = lax.axis_index("tp")
    chips = tp // 2
    casts = (up_cast, down_cast)
    alls = (up_all, down_all)
    outs = (up_out, down_out)
    tokens = rows_ref.shape[0]
    share = tokens // tp

    def source(device, j):
        return lax.rem(device // 2 + j // 2, chips) * 2 + lax.rem(lax.rem(device, 2) + j % 2, 2)

    def target(j):
        return lax.rem(me // 2 + chips - j // 2, chips) * 2 + lax.rem(lax.rem(me, 2) + j % 2, 2)

    def columns(w, b):
        width = casts[w].shape[2]
        return pl.ds(pl.multiple_of(b * width, width), width)

    def block(w, a, b, h):
        depth = casts[w].shape[1]
        half = depth // 2
        return alls[w].at[pl.ds(pl.multiple_of(a * depth + h * half, half), half), columns(w, b)]

    def remote(src, dst, send, recv, device):
        return pltpu.make_async_remote_copy(
            src_ref=src, dst_ref=dst, send_sem=send, recv_sem=recv,
            device_id=device, device_id_type=MESH,
        )

    def tp_copy(w, j, k):
        h = y if k == 0 else 1 - y
        half = casts[w].shape[1] // 2
        t = target(j)
        src = casts[w].at[t, pl.ds(pl.multiple_of(h * half, half), half), :]
        return remote(src, block(w, z, me, h), tp_send.at[w, j, k], tp_recv.at[w, j, k], {"tp": t})

    def tp_arrival(w, j, k):
        h = y if k == 0 else 1 - y
        ref = block(w, z, source(me, j), h)
        return remote(ref, ref, tp_send.at[w, j, k], tp_recv.at[w, j, k], {"tp": target(j)})

    def z_copy(w, j, a, slot, device):
        ref = block(w, a, source(me, j), y)
        return remote(ref, ref, z_send.at[w, j, slot], z_recv.at[w, j, a], {"fs": device})

    def y_copy(w, j, a, h):
        ref = block(w, a, source(me, j), h)
        return remote(ref, ref, y_send.at[w, j, a], y_recv.at[w, j, a], {"grp": 1 - y})

    def local_copy(w):
        depth = casts[w].shape[1]
        dst = alls[w].at[pl.ds(pl.multiple_of(z * depth, depth), depth), columns(w, me)]
        return pltpu.make_async_copy(casts[w].at[me], dst, local_sem.at[w])

    def out_copy(w, j):
        cols = columns(w, source(me, j))
        return pltpu.make_async_copy(alls[w].at[:, cols], outs[w].at[:, cols], out_sem.at[w, j])

    def sum_copy(j, k):
        t = target(k)
        cols = columns(1, source(me, j))
        src = part.at[pl.ds(pl.multiple_of(t * share, share), share), cols]
        return remote(src, arrived.at[k - 1, :, cols], sum_send.at[j, k], sum_recv.at[j, k], {"tp": t})

    def sum_arrival(j, k):
        cols = columns(1, source(source(me, k), j))
        ref = arrived.at[k - 1, :, cols]
        return remote(ref, ref, sum_send.at[j, k], sum_recv.at[j, k], {"tp": target(k)})

    barrier = pltpu.get_barrier_semaphore()
    for j in range(1, tp):
        pl.semaphore_signal(barrier, inc=1, device_id={"tp": target(j)}, device_id_type=MESH)
    pl.semaphore_signal(barrier, inc=1, device_id={"grp": 1 - y}, device_id_type=MESH)

    @pl.when(z > 0)
    def _():
        pl.semaphore_signal(barrier, inc=1, device_id={"fs": z - 1}, device_id_type=MESH)

    @pl.when(z < n - 1)
    def _():
        pl.semaphore_signal(barrier, inc=1, device_id={"fs": z + 1}, device_id_type=MESH)

    for w in range(2):
        local_copy(w).start()
    pl.semaphore_wait(barrier, tp + (z + n - 1) // n + (2 * n - 2 - z) // n)

    for w in range(2):
        for k in range(2):
            for j in range(1, tp):
                tp_copy(w, j, k).start()

    def own_send(w, j):
        if j == 0:
            local_copy(w).wait()
        else:
            tp_arrival(w, j, 0).wait_recv()

        @pl.when(z < n - 1)
        def _():
            z_copy(w, j, z, z, z + 1).start()

        @pl.when(z > 0)
        def _():
            z_copy(w, j, z, n, z - 1).start()

    def process(w, j):
        for s in range(1, n):

            @pl.when(z - s >= 0)
            def _():
                a = z - s
                z_copy(w, j, a, a, z).wait_recv()

                @pl.when(z < n - 1)
                def _():
                    z_copy(w, j, a, a, z + 1).start()

                y_copy(w, j, a, y).start()

            @pl.when(z + s < n)
            def _():
                a = z + s
                z_copy(w, j, a, a, z).wait_recv()

                @pl.when(z > 0)
                def _():
                    z_copy(w, j, a, a, z - 1).start()

                y_copy(w, j, a, y).start()

    def finish(w, j):
        if j > 0:
            tp_arrival(w, j, 1).wait_recv()
        for a in range(n):

            @pl.when(z != a)
            def _():
                y_copy(w, j, a, 1 - y).wait_recv()

        cols = columns(w, source(me, j))
        out_copy(w, j).start()

        @pl.loop(0, tokens // row_tile)
        def _(m):
            here = pl.ds(pl.multiple_of(m * row_tile, row_tile), row_tile)
            if w == 0:
                acc = jnp.dot(normed[here, :], up_all[:, cols], preferred_element_type=jnp.float32)
                acc = jnp.maximum(acc, 0.0)
                hidden[here, cols] = (acc * acc).astype(jnp.bfloat16)
            else:
                acc = jnp.dot(hidden[here, :], down_all[:, cols], preferred_element_type=jnp.float32)
                part[here, cols] = acc.astype(jnp.bfloat16)

        if w == 1:
            for k in range(1, tp):
                sum_copy(j, k).start()

    groups = [(w, j) for w in range(2) for j in range(tp)]
    own_send(*groups[0])
    own_send(*groups[1])

    @pl.loop(0, tokens // norm_tile)
    def _(m):
        here = pl.ds(pl.multiple_of(m * norm_tile, norm_tile), norm_tile)
        values = rows_ref[here, :].astype(jnp.float32)
        scale = lax.rsqrt(jnp.mean(values * values, axis=-1, keepdims=True) + eps)
        normed[here, :] = (values * scale).astype(jnp.bfloat16)

    for g in range(len(groups)):
        process(*groups[g])
        if g + 2 < len(groups):
            own_send(*groups[g + 2])
        if g >= 1:
            finish(*groups[g - 1])
    finish(*groups[-1])

    for j in range(tp):
        for k in range(1, tp):
            sum_arrival(j, k).wait_recv()

    @pl.loop(0, share // norm_tile)
    def _(m):
        here = pl.ds(pl.multiple_of(m * norm_tile, norm_tile), norm_tile)
        mine = pl.ds(pl.multiple_of(me * share + m * norm_tile, norm_tile), norm_tile)
        total = part[mine, :].astype(jnp.float32)
        for k in range(tp - 1):
            total = total + arrived[k, here, :].astype(jnp.float32)
        layer_out[here, :] = total.astype(jnp.bfloat16)

    for w in range(2):
        for j in range(tp):
            out_copy(w, j).wait()
            if j > 0:
                for k in range(2):
                    tp_copy(w, j, k).wait_send()

            @pl.when(z > 0)
            def _():
                z_copy(w, j, z, n, z - 1).wait_send()

            for a in range(n):

                @pl.when(jnp.logical_and(a <= z, z < n - 1))
                def _():
                    z_copy(w, j, a, a, z + 1).wait_send()

                @pl.when(jnp.logical_and(a > z, z > 0))
                def _():
                    z_copy(w, j, a, a, z - 1).wait_send()

                @pl.when(z != a)
                def _():
                    y_copy(w, j, a, y).wait_send()

    for j in range(tp):
        for k in range(1, tp):
            sum_copy(j, k).wait_send()


def place_kernel(up_in, down_in, up_out, down_out, slots, in_sem, out_sem):
    jobs = []
    for src, dst in ((up_in, up_out), (down_in, down_out)):
        for first in range(0, src.shape[0], copy_rows):
            jobs.append((src.at[first : first + copy_rows, :], dst.at[first : first + copy_rows, :]))

    def load(i):
        slot = i % copy_slots
        here = slots.at[slot, :, : jobs[i][0].shape[1]]
        return pltpu.make_async_copy(jobs[i][0], here, in_sem.at[slot])

    def store(i):
        slot = i % copy_slots
        here = slots.at[slot, :, : jobs[i][0].shape[1]]
        return pltpu.make_async_copy(here, jobs[i][1], out_sem.at[slot])

    count = len(jobs)
    ahead = copy_slots // 2
    for i in range(count + ahead):
        if i < count:
            if i >= copy_slots:
                store(i - copy_slots).wait()
            load(i).start()
        if i >= ahead:
            load(i - ahead).wait()
            store(i - ahead).start()
    for i in range(max(0, count - copy_slots), count):
        store(i).wait()


def on_device(prompt_rows, up_master, down_master, norm_gain):
    n = lax.axis_size("fs")
    tp = lax.axis_size("tp")
    bf16 = jnp.bfloat16
    up_rows, width = up_master.shape
    span = width // n
    fs_per_tp = n // tp
    up_width = fs_per_tp * span
    down_width = down_master.shape[1]
    up_cast = (up_master * norm_gain[:, None]).astype(bf16)
    up_cast = up_cast.reshape(up_rows, fs_per_tp, tp, span).transpose(2, 0, 1, 3)
    up_cast = up_cast.reshape(tp, up_rows, up_width)
    down_cast = down_master.astype(bf16).reshape(tp, down_master.shape[0] // tp, down_width)
    tokens, model = prompt_rows.shape
    units = n * span
    share = tokens // tp
    vmem = pl.BlockSpec(memory_space=pltpu.VMEM)
    hbm = pl.BlockSpec(memory_space=pl.ANY)
    dma = pltpu.SemaphoreType.DMA
    up_shape = jax.ShapeDtypeStruct((model, units), bf16)
    down_shape = jax.ShapeDtypeStruct((units, model), bf16)
    up_all, down_all, layer_out = pl.pallas_call(
        functools.partial(gather_kernel, n, tp),
        out_shape=(up_shape, down_shape, jax.ShapeDtypeStruct((share, model), bf16)),
        in_specs=[vmem, vmem, vmem],
        out_specs=(hbm, hbm, vmem),
        scratch_shapes=[
            pltpu.VMEM((model, units), bf16),
            pltpu.VMEM((units, model), bf16),
            pltpu.VMEM((tokens, model), bf16),
            pltpu.VMEM((tokens, units), bf16),
            pltpu.VMEM((tokens, model), bf16),
            pltpu.VMEM((tp - 1, share, model), bf16),
            dma((2,)),
            dma((2, tp, 2)),
            dma((2, tp, 2)),
            dma((2, tp, n + 1)),
            dma((2, tp, n)),
            dma((2, tp, n)),
            dma((2, tp, n)),
            dma((tp, tp)),
            dma((tp, tp)),
            dma((2, tp)),
        ],
        compiler_params=pltpu.CompilerParams(
            collective_id=0, has_side_effects=True, vmem_limit_bytes=60 * 1024 * 1024
        ),
    )(up_cast, down_cast, prompt_rows)
    up_sampler, down_sampler = pl.pallas_call(
        place_kernel,
        out_shape=(up_shape, down_shape),
        in_specs=[hbm, hbm],
        out_specs=(hbm, hbm),
        scratch_shapes=[
            pltpu.VMEM((copy_slots, copy_rows, max(model, units)), bf16),
            dma((copy_slots,)),
            dma((copy_slots,)),
        ],
    )(up_all, down_all)
    return (up_sampler[None], down_sampler[None], layer_out)


def solution(mesh):
    in_specs = (P(("grp", "fs"), None), P("fs", "tp"), P("fs", "tp"), P("fs"))
    out_specs = (
        P(("grp", "tp"), None, None),
        P(("grp", "tp"), None, None),
        P(("grp", "fs", "tp"), None),
    )
    return jax.shard_map(
        on_device, mesh=mesh, in_specs=in_specs, out_specs=out_specs, check_vma=False
    )
```

time: 418 us -> 203 us (0.49)
  waiting for transfers between devices: 273 us -> 0 us
  Pallas kernels: 0 us -> 187 us
  blocking collectives: 58.7 us -> 0 us
  local copies, waits for them, and re-layouts: 36.7 us -> 8.69 us
  matrix products: 25.4 us -> 0 us
  between operations: 13.8 us -> 0.67 us
    all_gather x2 -> x0, waiting for transfers between devices: 254 us -> none  [the longest x1 150 us: on_device(): up_sampler = lax.all_gather(up_local, 'fs', axis=0, tiled=True)]
    pallas_call x0 -> x2, Pallas kernels: none -> 187 us  [the longest x1 174 us: on_device(): pl.pallas_call(functools.partial(gather_kernel, n, tp), out_shape=(up_sha...]
    all_to_all x2 -> x0, blocking collectives: 58.7 us -> none  [the longest x1 30 us: on_device(): lax.all_to_all(up_parts, 'tp', split_axis=2, concat_axis=1, tiled=True)]
    dot_general x1 -> x0, matrix products: 25.4 us -> none  [on_device(): jnp.dot(hidden, down_sampler, preferred_element_type=jnp.float32)]
    unnamed x5 -> x6, local copies, waits for them, and re-layouts: 29.6 us -> 6.33 us
    reduce_scatter x1 -> x0, waiting for transfers between devices: 18.4 us -> none  [on_device(): lax.psum_scatter(jnp.dot(hidden, down_sampler, preferred_element_type=jnp...]
    all_to_all x2 -> x0, local copies, waits for them, and re-layouts: 4.71 us -> none  [the longest x1 2.35 us: on_device(): lax.all_to_all(down_parts, 'tp', split_axis=0, concat_axis=2, tiled=True)]
  transfers between devices with their start and end apart: 3 -> 0, of which waited for: 3 -> 0; matrix products, arithmetic and copies ran while one was open for 10% -> 0% of each run, Pallas kernels for 0% -> 0%
where the time goes in v1:
time: 203 us
  Pallas kernels  187 us (92%)
  local copies, waits for them, and re-layouts  8.69 us (4%)
  other arithmetic  6.54 us (3%)
    pallas_call x1, Pallas kernels, on_device(): pl.pallas_call(functools.partial(gather_kernel, n, tp), out_shape=(up_sha...  174 us
    pallas_call x1, Pallas kernels, on_device(): pl.pallas_call(place_kernel, out_shape=(up_shape, down_shape), in_specs=[...  12.5 us
    unnamed x6, local copies, waits for them, and re-layouts  6.33 us

profile of v1, /device:TPU:1, one launch (start us, length us, event | category | flops | bytes accessed | tf_op | source)
XLA Modules:
  0.0 202.9 jit_solution(13320985404812884875)
XLA Ops:
  0.6 3.8 %convert_element_type.7 = bf16[2048,512]{1,0:T(8,128)(2,1)} convert(f32[2048,512]{1,0:T(8,128)} %param.6) | non-fusion elementwise | flops 1048576 | bytes 6291456 | tf_op jit(solution)/shard_map/convert_element_type | solution.py:287
  4.4 0.0 copy-start.1
  4.4 5.3 %copy.7 = f32[512,2048]{0,1:T(8,128)} copy(f32[512,2048]{1,0:T(8,128)} %param.5) | data formatting | bytes 8388608 | tf_op args[1]
  9.8 0.0 copy-done.1
  9.8 2.8 %multiply_convert_fusion = bf16[512,2048]{0,1:T(8,128)(2,1)S(1)} fusion(f32[512,2048]{0,1:T(8,128)} %copy.7, f32[512]{0:T(512)S(1)} %copy-done.1), kind=kLoop, calls=%fused_computation | loop fusion | flops 2097152 | bytes 6293504 | tf_op jit(solution)/shard_map/convert_element_type | solution.py:284
  12.5 2.4 %copy.8 = bf16[512,1,4,512]{3,0,2,1:T(8,128)(2,1)} copy(bf16[512,1,4,512]{0,3,2,1:T(8,128)(2,1)S(1)} %bitcast.8) | data formatting | bytes 4194304 | tf_op jit(solution)/shard_map/reshape | solution.py:285
  14.9 174.5 %shard_map.67 = (bf16[2048,2048]{1,0:T(8,128)(2,1)}, bf16[2048,2048]{1,0:T(8,128)(2,1)}, bf16[256,2048]{1,0:T(8,128)(2,1)}) custom-call(bf16[4,512,512]{2,1,0:T(8,128)(2,1)} %bitcast.9, bf16[4,512,512]{2,1,0:T(8,128)(2,1)} %bitcast.7, bf16[1024,2048]{1,0:T(8,128)(2,1)} %rows_ref.1), custom_call_target="tpu_custom_call" | custom-call | tf_op jit(solution)/shard_map/pallas_call | solution.py:296
  189.4 0.0 copy-start
  189.4 12.5 %shard_map.68 = (bf16[2048,2048]{1,0:T(8,128)(2,1)}, bf16[2048,2048]{1,0:T(8,128)(2,1)}) custom-call(bf16[2048,2048]{1,0:T(8,128)(2,1)} %get-tuple-element.8.up_in, bf16[2048,2048]{1,0:T(8,128)(2,1)} %get-tuple-element.9.down_in), custom_call_target="tpu_custom_call" | custom-call | tf_op jit(solution)/shard_map/pallas_call | solution.py:323
  201.9 0.0 copy-done
  201.9 1.0 copy.10
Async XLA Ops:
  4.4 5.4 %copy-start.1 = (f32[512]{0:T(512)S(1)}, f32[512]{0:T(512)}, u32[]{:S(2)}) copy-start(f32[512]{0:T(512)} %param.7) | copy-start | bytes 6148
  189.4 12.5 %copy-start = (bf16[256,2048]{1,0:T(8,128)(2,1)S(1)}, bf16[256,2048]{1,0:T(8,128)(2,1)}, u32[]{:S(2)}) copy-start(bf16[256,2048]{1,0:T(8,128)(2,1)} %get-tuple-element.18) | copy-start | bytes 3145732

commit v2 on v1

--- a/solution.py
+++ b/solution.py
@@ -16,8 +16,9 @@
 
 
 def gather_kernel(
-    n, tp, up_cast, down_cast, rows_ref, up_out, down_out, layer_out,
+    n, tp, cuts, up_ref, down_ref, gain_ref, rows_ref, up_out, down_out, layer_out,
     up_all, down_all, normed, hidden, part, arrived,
+    up_stage, down_stage, up_cast, down_cast, gain_tall, load_sem,
     local_sem, tp_send, tp_recv, z_send, z_recv, y_send, y_recv,
     sum_send, sum_recv, out_sem,
 ):
@@ -25,7 +26,8 @@
     z = lax.axis_index("fs")
     me = lax.axis_index("tp")
     chips = tp // 2
-    casts = (up_cast, down_cast)
+    depths = (up_ref.shape[0], down_ref.shape[0] // tp)
+    widths = (up_ref.shape[1] // tp, down_ref.shape[1])
     alls = (up_all, down_all)
     outs = (up_out, down_out)
     tokens = rows_ref.shape[0]
@@ -37,14 +39,21 @@
     def target(j):
         return lax.rem(me // 2 + chips - j // 2, chips) * 2 + lax.rem(lax.rem(me, 2) + j % 2, 2)
 
-    def columns(w, b):
-        width = casts[w].shape[2]
-        return pl.ds(pl.multiple_of(b * width, width), width)
-
-    def block(w, a, b, h):
-        depth = casts[w].shape[1]
-        half = depth // 2
-        return alls[w].at[pl.ds(pl.multiple_of(a * depth + h * half, half), half), columns(w, b)]
+    def columns(w, b, i=None):
+        if i is None:
+            return pl.ds(pl.multiple_of(b * widths[w], widths[w]), widths[w])
+        width = widths[w] // cuts
+        return pl.ds(pl.multiple_of(b * widths[w] + i * width, width), width)
+
+    def block(w, a, b, h, i=None):
+        half = depths[w] // 2
+        first = a * depths[w] + h * half
+        return alls[w].at[pl.ds(pl.multiple_of(first, half), half), columns(w, b, i)]
+
+    def cast_block(w, t, first, count):
+        if w == 0:
+            return up_cast.at[pl.ds(pl.multiple_of(first, count), count), columns(0, t)]
+        return down_cast.at[pl.ds(pl.multiple_of(t * depths[1] + first, count), count), :]
 
     def remote(src, dst, send, recv, device):
         return pltpu.make_async_remote_copy(
@@ -54,9 +63,9 @@
 
     def tp_copy(w, j, k):
         h = y if k == 0 else 1 - y
-        half = casts[w].shape[1] // 2
+        half = depths[w] // 2
         t = target(j)
-        src = casts[w].at[t, pl.ds(pl.multiple_of(h * half, half), half), :]
+        src = cast_block(w, t, h * half, half)
         return remote(src, block(w, z, me, h), tp_send.at[w, j, k], tp_recv.at[w, j, k], {"tp": t})
 
     def tp_arrival(w, j, k):
@@ -64,18 +73,18 @@
         ref = block(w, z, source(me, j), h)
         return remote(ref, ref, tp_send.at[w, j, k], tp_recv.at[w, j, k], {"tp": target(j)})
 
-    def z_copy(w, j, a, slot, device):
-        ref = block(w, a, source(me, j), y)
-        return remote(ref, ref, z_send.at[w, j, slot], z_recv.at[w, j, a], {"fs": device})
-
-    def y_copy(w, j, a, h):
-        ref = block(w, a, source(me, j), h)
-        return remote(ref, ref, y_send.at[w, j, a], y_recv.at[w, j, a], {"grp": 1 - y})
+    def z_copy(w, g, a, slot, device):
+        ref = block(w, a, source(me, g // cuts), y, g % cuts)
+        return remote(ref, ref, z_send.at[w, g, slot], z_recv.at[w, g, a], {"fs": device})
+
+    def y_copy(w, g, a, h):
+        ref = block(w, a, source(me, g // cuts), h, g % cuts)
+        return remote(ref, ref, y_send.at[w, g, a], y_recv.at[w, g, a], {"grp": 1 - y})
 
     def local_copy(w):
-        depth = casts[w].shape[1]
+        depth = depths[w]
         dst = alls[w].at[pl.ds(pl.multiple_of(z * depth, depth), depth), columns(w, me)]
-        return pltpu.make_async_copy(casts[w].at[me], dst, local_sem.at[w])
+        return pltpu.make_async_copy(cast_block(w, me, 0, depth), dst, local_sem.at[w])
 
     def out_copy(w, j):
         cols = columns(w, source(me, j))
@@ -83,15 +92,25 @@
 
     def sum_copy(j, k):
         t = target(k)
-        cols = columns(1, source(me, j))
+        cols = columns(1, source(me, j // cuts), j % cuts)
         src = part.at[pl.ds(pl.multiple_of(t * share, share), share), cols]
         return remote(src, arrived.at[k - 1, :, cols], sum_send.at[j, k], sum_recv.at[j, k], {"tp": t})
 
     def sum_arrival(j, k):
-        cols = columns(1, source(source(me, k), j))
+        cols = columns(1, source(source(me, k), j // cuts), j % cuts)
         ref = arrived.at[k - 1, :, cols]
         return remote(ref, ref, sum_send.at[j, k], sum_recv.at[j, k], {"tp": target(k)})
 
+    def up_load(h, k):
+        here = pl.ds(pl.multiple_of(h * (depths[0] // 2), depths[0] // 2), depths[0] // 2)
+        return pltpu.make_async_copy(up_ref.at[here, :], up_stage.at[here, :], load_sem.at[k])
+
+    down_load = pltpu.make_async_copy(down_ref, down_stage, load_sem.at[2])
+    rows_load = pltpu.make_async_copy(rows_ref, normed, load_sem.at[3])
+    up_load(y, 0).start()
+    up_load(1 - y, 1).start()
+    down_load.start()
+    rows_load.start()
     barrier = pltpu.get_barrier_semaphore()
     for j in range(1, tp):
         pl.semaphore_signal(barrier, inc=1, device_id={"tp": target(j)}, device_id_type=MESH)
@@ -105,20 +124,27 @@
     def _():
         pl.semaphore_signal(barrier, inc=1, device_id={"fs": z + 1}, device_id_type=MESH)
 
-    for w in range(2):
-        local_copy(w).start()
+    half = depths[0] // 2
+    gain_tall[...] = jnp.broadcast_to(gain_ref[...], (128, depths[0])).T
+
+    @pl.loop(0, 2)
+    def _(k):
+        h = y + k - 2 * y * k
+        start = pl.multiple_of(h * half, half)
+        up_load(h, k).wait()
+
+        @pl.loop(0, half // norm_tile)
+        def _(m):
+            here = pl.ds(pl.multiple_of(start + m * norm_tile, norm_tile), norm_tile)
+            up_cast[here, :] = (up_stage[here, :] * gain_tall[here, :1]).astype(jnp.bfloat16)
+
     pl.semaphore_wait(barrier, tp + (z + n - 1) // n + (2 * n - 2 - z) // n)
-
-    for w in range(2):
-        for k in range(2):
-            for j in range(1, tp):
-                tp_copy(w, j, k).start()
 
     def own_send(w, j):
         if j == 0:
             local_copy(w).wait()
-        else:
-            tp_arrival(w, j, 0).wait_recv()
+        elif j % cuts == 0:
+            tp_arrival(w, j // cuts, 0).wait_recv()
 
         @pl.when(z < n - 1)
         def _():
@@ -154,16 +180,17 @@
                 y_copy(w, j, a, y).start()
 
     def finish(w, j):
-        if j > 0:
-            tp_arrival(w, j, 1).wait_recv()
+        if j > 0 and j % cuts == 0:
+            tp_arrival(w, j // cuts, 1).wait_recv()
         for a in range(n):
 
             @pl.when(z != a)
             def _():
                 y_copy(w, j, a, 1 - y).wait_recv()
 
-        cols = columns(w, source(me, j))
-        out_copy(w, j).start()
+        cols = columns(w, source(me, j // cuts), j % cuts)
+        if j % cuts == cuts - 1:
+            out_copy(w, j // cuts).start()
 
         @pl.loop(0, tokens // row_tile)
         def _(m):
@@ -180,26 +207,47 @@
             for k in range(1, tp):
                 sum_copy(j, k).start()
 
-    groups = [(w, j) for w in range(2) for j in range(tp)]
-    own_send(*groups[0])
-    own_send(*groups[1])
+    def exchange(w, k):
+        for j in range(1, tp):
+            tp_copy(w, j, k).start()
+
+    groups = [(w, j) for w in range(2) for j in range(tp * cuts)]
+    exchange(0, 0)
+    local_copy(0).start()
+    for g in range(cuts):
+        own_send(*groups[g])
+    exchange(0, 1)
+    down_load.wait()
+
+    @pl.loop(0, down_ref.shape[0] // norm_tile)
+    def _(m):
+        here = pl.ds(pl.multiple_of(m * norm_tile, norm_tile), norm_tile)
+        down_cast[here, :] = down_stage[here, :].astype(jnp.bfloat16)
+
+    rows_load.wait()
 
     @pl.loop(0, tokens // norm_tile)
     def _(m):
         here = pl.ds(pl.multiple_of(m * norm_tile, norm_tile), norm_tile)
-        values = rows_ref[here, :].astype(jnp.float32)
+        values = normed[here, :].astype(jnp.float32)
         scale = lax.rsqrt(jnp.mean(values * values, axis=-1, keepdims=True) + eps)
         normed[here, :] = (values * scale).astype(jnp.bfloat16)
 
+    exchange(1, 0)
+    exchange(1, 1)
+    local_copy(1).start()
+    ahead = 3
+    for g in range(cuts, ahead):
+        own_send(*groups[g])
     for g in range(len(groups)):
         process(*groups[g])
-        if g + 2 < len(groups):
-            own_send(*groups[g + 2])
+        if g + ahead < len(groups):
+            own_send(*groups[g + ahead])
         if g >= 1:
             finish(*groups[g - 1])
     finish(*groups[-1])
 
-    for j in range(tp):
+    for j in range(tp * cuts):
         for k in range(1, tp):
             sum_arrival(j, k).wait_recv()
 
@@ -218,6 +266,7 @@
             if j > 0:
                 for k in range(2):
                     tp_copy(w, j, k).wait_send()
+        for j in range(tp * cuts):
 
             @pl.when(z > 0)
             def _():
@@ -237,7 +286,7 @@
                 def _():
                     y_copy(w, j, a, y).wait_send()
 
-    for j in range(tp):
+    for j in range(tp * cuts):
         for k in range(1, tp):
             sum_copy(j, k).wait_send()
 
@@ -281,10 +330,10 @@
     fs_per_tp = n // tp
     up_width = fs_per_tp * span
     down_width = down_master.shape[1]
-    up_cast = (up_master * norm_gain[:, None]).astype(bf16)
-    up_cast = up_cast.reshape(up_rows, fs_per_tp, tp, span).transpose(2, 0, 1, 3)
-    up_cast = up_cast.reshape(tp, up_rows, up_width)
-    down_cast = down_master.astype(bf16).reshape(tp, down_master.shape[0] // tp, down_width)
+    if fs_per_tp > 1:
+        up_master = up_master.reshape(up_rows, fs_per_tp, tp, span).swapaxes(1, 2)
+        up_master = up_master.reshape(up_rows, width)
+    cuts = 2 if up_width % 256 == 0 and down_width % 256 == 0 else 1
     tokens, model = prompt_rows.shape
     units = n * span
     share = tokens // tp
@@ -294,9 +343,9 @@
     up_shape = jax.ShapeDtypeStruct((model, units), bf16)
     down_shape = jax.ShapeDtypeStruct((units, model), bf16)
     up_all, down_all, layer_out = pl.pallas_call(
-        functools.partial(gather_kernel, n, tp),
+        functools.partial(gather_kernel, n, tp, cuts),
         out_shape=(up_shape, down_shape, jax.ShapeDtypeStruct((share, model), bf16)),
-        in_specs=[vmem, vmem, vmem],
+        in_specs=[hbm, hbm, vmem, hbm],
         out_specs=(hbm, hbm, vmem),
         scratch_shapes=[
             pltpu.VMEM((model, units), bf16),
@@ -305,21 +354,27 @@
             pltpu.VMEM((tokens, units), bf16),
             pltpu.VMEM((tokens, model), bf16),
             pltpu.VMEM((tp - 1, share, model), bf16),
+            pltpu.VMEM(up_master.shape, jnp.float32),
+            pltpu.VMEM(down_master.shape, jnp.float32),
+            pltpu.VMEM(up_master.shape, bf16),
+            pltpu.VMEM(down_master.shape, bf16),
+            pltpu.VMEM((up_rows, 128), jnp.float32),
+            dma((4,)),
             dma((2,)),
             dma((2, tp, 2)),
             dma((2, tp, 2)),
-            dma((2, tp, n + 1)),
-            dma((2, tp, n)),
-            dma((2, tp, n)),
-            dma((2, tp, n)),
-            dma((tp, tp)),
-            dma((tp, tp)),
+            dma((2, tp * cuts, n + 1)),
+            dma((2, tp * cuts, n)),
+            dma((2, tp * cuts, n)),
+            dma((2, tp * cuts, n)),
+            dma((tp * cuts, tp)),
+            dma((tp * cuts, tp)),
             dma((2, tp)),
         ],
         compiler_params=pltpu.CompilerParams(
             collective_id=0, has_side_effects=True, vmem_limit_bytes=60 * 1024 * 1024
         ),
-    )(up_cast, down_cast, prompt_rows)
+    )(up_master, down_master, norm_gain[None, :], prompt_rows)
     up_sampler, down_sampler = pl.pallas_call(
         place_kernel,
         out_shape=(up_shape, down_shape),

time: 203 us -> 181 us (0.89)
  local copies, waits for them, and re-layouts: 8.69 us -> 0.98 us
  Pallas kernels: 187 us -> 180 us
  other arithmetic: 6.54 us -> 0 us
    pallas_call x1, Pallas kernels: 174 us -> 167 us  [on_device(): pl.pallas_call(functools.partial(gather_kernel, n, tp, cuts), out_shape=(...]
    convert_element_type x2 -> x0, other arithmetic: 6.54 us -> none  [the longest x1 3.77 us: on_device(): down_master.astype(bf16).reshape(tp, down_master.shape[0] // tp, down_width)]
    unnamed x6 -> x3, local copies, waits for them, and re-layouts: 6.33 us -> 0.98 us
    reshape x1 -> x0, local copies, waits for them, and re-layouts: 2.36 us -> none  [on_device(): up_cast.reshape(up_rows, fs_per_tp, tp, span).transpose(2, 0, 1, 3)]
where the time goes in v2:
time: 181 us
  Pallas kernels  180 us (99%)
    pallas_call x1, Pallas kernels, on_device(): pl.pallas_call(functools.partial(gather_kernel, n, tp, cuts), out_shape=(...  167 us
    pallas_call x1, Pallas kernels, on_device(): pl.pallas_call(place_kernel, out_shape=(up_shape, down_shape), in_specs=[...  12.5 us

profile of v2, /device:TPU:1, one launch (start us, length us, event | category | flops | bytes accessed | tf_op | source)
XLA Modules:
  0.0 181.3 jit_solution(7383420248662280429)
XLA Ops:
  0.6 167.1 %shard_map.67 = (bf16[2048,2048]{1,0:T(8,128)(2,1)}, bf16[2048,2048]{1,0:T(8,128)(2,1)}, bf16[256,2048]{1,0:T(8,128)(2,1)}) custom-call(f32[512,2048]{1,0:T(8,128)} %up_ref.1, f32[2048,512]{1,0:T(8,128)} %down_ref.1, f32[1,512]{1,0:T(1,128)} %bitcast.3, bf16[1024,2048]{1,0:T(8,128)(2,1)} %rows_ref.1), custom_call_target="tpu_custom_call" | custom-call | tf_op jit(solution)/shard_map/pallas_call | solution.py:345
  167.7 0.0 copy-start
  167.8 12.5 %shard_map.68 = (bf16[2048,2048]{1,0:T(8,128)(2,1)}, bf16[2048,2048]{1,0:T(8,128)(2,1)}) custom-call(bf16[2048,2048]{1,0:T(8,128)(2,1)} %get-tuple-element.8.up_in, bf16[2048,2048]{1,0:T(8,128)(2,1)} %get-tuple-element.9.down_in), custom_call_target="tpu_custom_call" | custom-call | tf_op jit(solution)/shard_map/pallas_call | solution.py:378
  180.3 0.0 copy-done
  180.3 1.0 copy.8
Async XLA Ops:
  167.7 12.5 %copy-start = (bf16[256,2048]{1,0:T(8,128)(2,1)S(1)}, bf16[256,2048]{1,0:T(8,128)(2,1)}, u32[]{:S(2)}) copy-start(bf16[256,2048]{1,0:T(8,128)(2,1)} %get-tuple-element.18) | copy-start | bytes 3145732

commit v3 on v2

--- a/solution.py
+++ b/solution.py
@@ -11,7 +11,6 @@
 row_tile = 256
 norm_tile = 64
 copy_rows = 256
-copy_slots = 8
 MESH = pl.DeviceIdType.MESH
 
 
@@ -81,10 +80,11 @@
         ref = block(w, a, source(me, g // cuts), h, g % cuts)
         return remote(ref, ref, y_send.at[w, g, a], y_recv.at[w, g, a], {"grp": 1 - y})
 
-    def local_copy(w):
-        depth = depths[w]
-        dst = alls[w].at[pl.ds(pl.multiple_of(z * depth, depth), depth), columns(w, me)]
-        return pltpu.make_async_copy(cast_block(w, me, 0, depth), dst, local_sem.at[w])
+    def local_copy(w, k):
+        h = y if k == 0 else 1 - y
+        half = depths[w] // 2
+        src = cast_block(w, me, h * half, half)
+        return pltpu.make_async_copy(src, block(w, z, me, h), local_sem.at[w, k])
 
     def out_copy(w, j):
         cols = columns(w, source(me, j))
@@ -127,22 +127,23 @@
     half = depths[0] // 2
     gain_tall[...] = jnp.broadcast_to(gain_ref[...], (128, depths[0])).T
 
-    @pl.loop(0, 2)
-    def _(k):
-        h = y + k - 2 * y * k
-        start = pl.multiple_of(h * half, half)
+    def cast_half(k):
+        h = y if k == 0 else 1 - y
         up_load(h, k).wait()
 
         @pl.loop(0, half // norm_tile)
         def _(m):
-            here = pl.ds(pl.multiple_of(start + m * norm_tile, norm_tile), norm_tile)
+            first = h * half + m * norm_tile
+            here = pl.ds(pl.multiple_of(first, norm_tile), norm_tile)
             up_cast[here, :] = (up_stage[here, :] * gain_tall[here, :1]).astype(jnp.bfloat16)
 
+    cast_half(0)
+    local_copy(0, 0).start()
     pl.semaphore_wait(barrier, tp + (z + n - 1) // n + (2 * n - 2 - z) // n)
 
     def own_send(w, j):
         if j == 0:
-            local_copy(w).wait()
+            local_copy(w, 0).wait()
         elif j % cuts == 0:
             tp_arrival(w, j // cuts, 0).wait_recv()
 
@@ -180,7 +181,9 @@
                 y_copy(w, j, a, y).start()
 
     def finish(w, j):
-        if j > 0 and j % cuts == 0:
+        if j == 0:
+            local_copy(w, 1).wait()
+        elif j % cuts == 0:
             tp_arrival(w, j // cuts, 1).wait_recv()
         for a in range(n):
 
@@ -213,9 +216,10 @@
 
     groups = [(w, j) for w in range(2) for j in range(tp * cuts)]
     exchange(0, 0)
-    local_copy(0).start()
     for g in range(cuts):
         own_send(*groups[g])
+    cast_half(1)
+    local_copy(0, 1).start()
     exchange(0, 1)
     down_load.wait()
 
@@ -235,7 +239,8 @@
 
     exchange(1, 0)
     exchange(1, 1)
-    local_copy(1).start()
+    local_copy(1, 0).start()
+    local_copy(1, 1).start()
     ahead = 3
     for g in range(cuts, ahead):
         own_send(*groups[g])
@@ -291,34 +296,27 @@
             sum_copy(j, k).wait_send()
 
 
-def place_kernel(up_in, down_in, up_out, down_out, slots, in_sem, out_sem):
-    jobs = []
-    for src, dst in ((up_in, up_out), (down_in, down_out)):
+def place_kernel(up_in, down_in, layer_in, up_out, down_out, layer_out, *scratch):
+    up_slots, down_slots, layer_slots, in_sem, out_sem = scratch
+    arrays = (
+        (up_in, up_slots, up_out),
+        (down_in, down_slots, down_out),
+        (layer_in, layer_slots, layer_out),
+    )
+    loads, stores = [], []
+    for src, slots, dst in arrays:
         for first in range(0, src.shape[0], copy_rows):
-            jobs.append((src.at[first : first + copy_rows, :], dst.at[first : first + copy_rows, :]))
-
-    def load(i):
-        slot = i % copy_slots
-        here = slots.at[slot, :, : jobs[i][0].shape[1]]
-        return pltpu.make_async_copy(jobs[i][0], here, in_sem.at[slot])
-
-    def store(i):
-        slot = i % copy_slots
-        here = slots.at[slot, :, : jobs[i][0].shape[1]]
-        return pltpu.make_async_copy(here, jobs[i][1], out_sem.at[slot])
-
-    count = len(jobs)
-    ahead = copy_slots // 2
-    for i in range(count + ahead):
-        if i < count:
-            if i >= copy_slots:
-                store(i - copy_slots).wait()
-            load(i).start()
-        if i >= ahead:
-            load(i - ahead).wait()
-            store(i - ahead).start()
-    for i in range(max(0, count - copy_slots), count):
-        store(i).wait()
+            here = slice(first, min(first + copy_rows, src.shape[0]))
+            i = len(loads)
+            loads.append(pltpu.make_async_copy(src.at[here, :], slots.at[here, :], in_sem.at[i]))
+            stores.append(pltpu.make_async_copy(slots.at[here, :], dst.at[here, :], out_sem.at[i]))
+    for load in loads:
+        load.start()
+    for load, store in zip(loads, stores):
+        load.wait()
+        store.start()
+    for store in stores:
+        store.wait()
 
 
 def on_device(prompt_rows, up_master, down_master, norm_gain):
@@ -360,7 +358,7 @@
             pltpu.VMEM(down_master.shape, bf16),
             pltpu.VMEM((up_rows, 128), jnp.float32),
             dma((4,)),
-            dma((2,)),
+            dma((2, 2)),
             dma((2, tp, 2)),
             dma((2, tp, 2)),
             dma((2, tp * cuts, n + 1)),
@@ -375,17 +373,20 @@
             collective_id=0, has_side_effects=True, vmem_limit_bytes=60 * 1024 * 1024
         ),
     )(up_master, down_master, norm_gain[None, :], prompt_rows)
-    up_sampler, down_sampler = pl.pallas_call(
+    layer_shape = jax.ShapeDtypeStruct((share, model), bf16)
+    moved = (up_shape, down_shape, layer_shape)
+    jobs = sum(-(-shape.shape[0] // copy_rows) for shape in moved)
+    up_sampler, down_sampler, layer_out = pl.pallas_call(
         place_kernel,
-        out_shape=(up_shape, down_shape),
-        in_specs=[hbm, hbm],
-        out_specs=(hbm, hbm),
+        out_shape=moved,
+        in_specs=[hbm, hbm, hbm],
+        out_specs=(hbm, hbm, hbm),
         scratch_shapes=[
-            pltpu.VMEM((copy_slots, copy_rows, max(model, units)), bf16),
-            dma((copy_slots,)),
-            dma((copy_slots,)),
+            *(pltpu.VMEM(shape.shape, bf16) for shape in moved),
+            dma((jobs,)),
+            dma((jobs,)),
         ],
-    )(up_all, down_all)
+    )(up_all, down_all, layer_out)
     return (up_sampler[None], down_sampler[None], layer_out)
 
 

time: 181 us -> 181 us (level)
  no operation moved by 1% of the time
where the time goes in v3:
time: 181 us
  Pallas kernels  180 us (99%)
    pallas_call x1, Pallas kernels, on_device(): pl.pallas_call(functools.partial(gather_kernel, n, tp, cuts), out_shape=(...  167 us
    pallas_call x1, Pallas kernels, on_device(): pl.pallas_call(place_kernel, out_shape=moved, in_specs=[hbm, hbm, hbm], o...  12.7 us

profile of v3, /device:TPU:1, one launch (start us, length us, event | category | flops | bytes accessed | tf_op | source)
XLA Modules:
  0.0 180.8 jit_solution(10552436475172593423)
XLA Ops:
  0.6 167.5 %shard_map.67 = (bf16[2048,2048]{1,0:T(8,128)(2,1)}, bf16[2048,2048]{1,0:T(8,128)(2,1)}, bf16[256,2048]{1,0:T(8,128)(2,1)}) custom-call(f32[512,2048]{1,0:T(8,128)} %up_ref.1, f32[2048,512]{1,0:T(8,128)} %down_ref.1, f32[1,512]{1,0:T(1,128)} %bitcast.3, bf16[1024,2048]{1,0:T(8,128)(2,1)} %rows_ref.1), custom_call_target="tpu_custom_call" | custom-call | tf_op jit(solution)/shard_map/pallas_call | solution.py:343
  168.1 12.7 %shard_map.68 = (bf16[2048,2048]{1,0:T(8,128)(2,1)}, bf16[2048,2048]{1,0:T(8,128)(2,1)}, bf16[256,2048]{1,0:T(8,128)(2,1)}) custom-call(bf16[2048,2048]{1,0:T(8,128)(2,1)} %get-tuple-element.9.up_in, bf16[2048,2048]{1,0:T(8,128)(2,1)} %get-tuple-element.10.down_in, bf16[256,2048]{1,0:T(8,128)(2,1)} %get-tuple-element.11.layer_in), custom_call_target="tpu_custom_call" | custom-call | tf_op jit(solution)/shard_map/pallas_call | solution.py:379
